TPU v7x, 32 devices: a whole 2x2x4 slice. The times are simulated.
32 devices in a mesh: sp: 8 (over z, y), tp: 4 (over x, core).
Axes of the slice: x: 2, y: 2, z: 4, core: 2. Of those that a mesh axis runs over, the one named last changes fastest.
Arguments:
- tokens: bfloat16 [8192, 2048], P('sp'), may hold values from -6 to 6
- norm_gain: bfloat16 [2048], replicated, may hold values from 0.099609375 to 1.8984375
- value_proj: bfloat16 [2048, 1024], P('sp', 'tp'), may hold values from -0.125 to 0.125
- glu_proj: bfloat16 [2048, 1024], P('sp', 'tp'), may hold values from -0.125 to 0.125
- recur_proj: bfloat16 [2048, 1024], P('sp', 'tp'), may hold values from -0.125 to 0.125
- branch_proj: bfloat16 [2048, 1024], P('sp', 'tp'), may hold values from -0.125 to 0.125
- channelwise_filter_taps: bfloat16 [31, 1024], P(None, 'tp'), may hold values from -1 to 1
- group_gain: bfloat16 [1024], P('tp'), may hold values from 0.099609375 to 1.8984375
- short_kernel: bfloat16 [4, 1024], P(None, 'tp'), may hold values from -3 to 3
- decay_map: bfloat16 [16, 64, 64], P('tp'), may hold values from -0.75 to 0.75
- entry_gate_matrix: bfloat16 [16, 64, 64], P('tp'), may hold values from -0.75 to 0.75
- rate_param: float32 [1024], P('tp'), may hold values from 4.5 to 15, as said below
- extra_decay: float32 [8192, 1024], P('sp', 'tp'), may hold values from -1 to 0, as said below
- conv_out: bfloat16 [1024, 2048], P('tp', 'sp'), may hold values from -0.125 to 0.125
- recur_out: bfloat16 [1024, 2048], P('tp', 'sp'), may hold values from -0.125 to 0.125
Outputs:
- mixed: bfloat16 [8192, 2048], P(('sp', 'tp'))
Inputs may be any that keep to these rules, and one draw needn't show every extreme that they name: `rate_param`: a finite parameter of each channel. `extra_decay`: every entry is negative.
All inputs are finite; a program needn't handle non-finite values.
Results may differ from a plain program's by a relative error of at most 0.015.
Values may be sent and summed in bfloat16 or wider, within the bound.
A program may use at most 64 MiB of HBM per device.

v0:
```python
import jax
import jax.numpy as jnp
from jax import lax
from jax.sharding import PartitionSpec as P

GROUP_CH = 64
HEAD_CH = 64


eps = 1e-06
gate_scale = 8.0


def from_behind(value, axis, steps):
    count = lax.axis_size(axis)
    first, last = (max(0, -steps), min(count, count - steps))
    return lax.ppermute(value, axis, [(source, source + steps) for source in range(first, last)])


def prefix(part, axis, combine, identity):
    place = lax.axis_index(axis)
    gathered = jax.tree.map(lambda a: lax.all_gather(a, axis), part)
    state = jax.tree.map(lambda a, e: jnp.zeros_like(a) + jnp.asarray(e, a.dtype), part, identity)

    def one(hop, state):
        return combine(
            state, jax.tree.map(lambda a: lax.dynamic_index_in_dim(a, hop, 0, False), gathered)
        )

    return lax.fori_loop(0, place, one, state)


def causal_taps(previous, current, kernel):
    taps = kernel.shape[0]
    length = current.shape[0]
    joined = jnp.concatenate([previous, current], axis=0).astype(jnp.float32)
    kernel_float = kernel.astype(jnp.float32)
    total = jnp.zeros(current.shape, jnp.float32)
    for offset in range(taps):
        total = total + kernel_float[offset] * joined[offset : offset + length]
    return total


def merge_pair(earlier, later):
    return (earlier[0] * later[0], later[0] * earlier[1] + later[1])


def body(
    tokens,
    norm_gain,
    value_proj,
    glu_proj,
    recur_proj,
    branch_proj,
    channelwise_filter_taps,
    group_gain,
    short_kernel,
    decay_map,
    entry_gate_matrix,
    rate_param,
    extra_decay,
    conv_out,
    recur_out,
):
    f32 = jnp.float32
    local_rows = tokens.shape[0]
    x_float = tokens.astype(f32)
    scale = lax.rsqrt(jnp.mean(x_float * x_float, axis=-1, keepdims=True) + eps)
    normed = (x_float * scale * norm_gain.astype(f32)).astype(jnp.bfloat16)
    conv_width = value_proj.shape[1]
    recurrence_width = recur_proj.shape[1]
    pieces = (
        lax.all_gather(value_proj, "sp", axis=0, tiled=True),
        lax.all_gather(glu_proj, "sp", axis=0, tiled=True),
        lax.all_gather(recur_proj, "sp", axis=0, tiled=True),
        lax.all_gather(branch_proj, "sp", axis=0, tiled=True),
    )
    value_part, glu_part, rec_float, arm_portion = tuple(
        (jnp.dot(normed, piece, preferred_element_type=f32) for piece in pieces)
    )
    gated = (value_part * jax.nn.sigmoid(glu_part)).astype(jnp.bfloat16)
    rec_input = rec_float.astype(jnp.bfloat16)
    taps_wide = channelwise_filter_taps.shape[0]
    taps_short = short_kernel.shape[0]
    prev_gated, prev_input = from_behind(
        (gated[local_rows - taps_wide + 1 :], rec_input[local_rows - taps_short + 1 :]), "sp", 1
    )
    conv_sum = causal_taps(prev_gated, gated, channelwise_filter_taps)
    grouped = conv_sum.reshape(local_rows, conv_width // GROUP_CH, GROUP_CH)
    center = jnp.mean(grouped, axis=-1, keepdims=True)
    spread = grouped - center
    var = jnp.mean(spread * spread, axis=-1, keepdims=True)
    grouped = (spread * lax.rsqrt(var + eps)).reshape(local_rows, conv_width)
    y_conv = jax.nn.silu(grouped * group_gain.astype(f32)).astype(jnp.bfloat16)
    rec_conv = causal_taps(prev_input, rec_input, short_kernel).astype(jnp.bfloat16)
    heads_view = rec_conv.reshape(local_rows, decay_map.shape[0], HEAD_CH)
    recur_gate = jax.nn.sigmoid(
        jnp.einsum("shi,hij->shj", heads_view, decay_map, preferred_element_type=f32).reshape(
            local_rows, recurrence_width
        )
    )
    input_gate = jax.nn.sigmoid(
        jnp.einsum(
            "shi,hij->shj", heads_view, entry_gate_matrix, preferred_element_type=f32
        ).reshape(local_rows, recurrence_width)
    )
    log_decay = -gate_scale * recur_gate * jax.nn.softplus(-rate_param)[None, :] + extra_decay
    decay = jnp.exp(log_decay)
    drive = jnp.sqrt(-jnp.expm1(2.0 * log_decay)) * input_gate * rec_conv.astype(f32)
    running_decay, running_state = lax.associative_scan(merge_pair, (decay, drive), axis=0)
    last_decay = running_decay[local_rows - 1]
    last_state = running_state[local_rows - 1]
    incoming = prefix(
        (last_decay, last_state),
        "sp",
        merge_pair,
        (jnp.ones_like(last_decay), jnp.zeros_like(last_state)),
    )[1]
    state = running_state + running_decay * incoming[None, :]
    y_lru = (state * jax.nn.gelu(arm_portion, approximate=True)).astype(jnp.bfloat16)
    conv_rows, rec_rows = (
        lax.all_to_all(y_conv, "tp", split_axis=0, concat_axis=1, tiled=True),
        lax.all_to_all(y_lru, "tp", split_axis=0, concat_axis=1, tiled=True),
    )
    conv_slab, rec_slab = (
        lax.all_gather(conv_out, "tp", axis=0, tiled=True),
        lax.all_gather(recur_out, "tp", axis=0, tiled=True),
    )
    joined_rows = jnp.concatenate([conv_rows, rec_rows], axis=1)
    weight_slab = jnp.concatenate([conv_slab, rec_slab], axis=0)
    mixed = jnp.dot(
        joined_rows,
        lax.all_gather(weight_slab, "sp", axis=1, tiled=True),
        preferred_element_type=f32,
    )
    return mixed.astype(jnp.bfloat16)


def solution(mesh):
    in_specs = (
        P("sp", None),
        P(),
        P("sp", "tp"),
        P("sp", "tp"),
        P("sp", "tp"),
        P("sp", "tp"),
        P(None, "tp"),
        P("tp"),
        P(None, "tp"),
        P("tp", None, None),
        P("tp", None, None),
        P("tp"),
        P("sp", "tp"),
        P("tp", "sp"),
        P("tp", "sp"),
    )
    out_specs = P(("sp", "tp"), None)
    return jax.shard_map(body, mesh=mesh, in_specs=in_specs, out_specs=out_specs, check_vma=False)
```

profile of v0, /device:TPU:0, one launch (start us, length us, event | category | flops | bytes accessed | tf_op | source)
XLA Modules:
  0.0 350.7 jit_solution(11380902504936581416)
XLA Ops:
  9.4 8.9 %all_gather.33 = bf16[1024,256]{1,0:T(8,128)(2,1)S(1)} all-gather(bf16[256,256]{1,0:T(8,128)(2,1)} %param.30), channel_id=1, replica_groups=mesh['sp'=8,'tp'=4] {'tp'}, dimensions={0}, use_global_device_ids=true | all-gather | bytes 655360 | tf_op jit(solution)/shard_map/all_gather | solution.py:126
  18.2 7.6 %all_gather.34 = bf16[1024,256]{1,0:T(8,128)(2,1)S(1)} all-gather(bf16[256,256]{1,0:T(8,128)(2,1)} %param.31), channel_id=1, replica_groups=mesh['sp'=8,'tp'=4] {'tp'}, dimensions={0}, use_global_device_ids=true | all-gather | bytes 655360 | tf_op jit(solution)/shard_map/all_gather | solution.py:127
  28.3 3.1 fusion
  32.0 5.3 %fusion.2 = bf16[1024,2048]{1,0:T(8,128)(2,1)} fusion(bf16[1024,2048]{1,0:T(8,128)(2,1)} %param.17, f32[2048]{0:T(1024)S(1)} %convert_element_type.47, f32[1024]{0:T(1024)S(1)} %add_rsqrt_fusion.1), kind=kLoop, calls=%fused_computation.7 | loop fusion | flops 8388608 | bytes 8400896 | tf_op jit(solution)/shard_map/convert_element_type | solution.py:69
  37.3 15.1 %all-gather.12.cloned.1.call-done = bf16[2048,256]{1,0:T(8,128)(2,1)} async-done(((bf16[256,256]{1,0:T(8,128)(2,1)}), bf16[2048,256]{1,0:T(8,128)(2,1)}) %all-gather.12.cloned.1.call-update) | async-done | bytes 1048592 | tf_op jit(solution)/shard_map/all_gather | solution.py:75
  52.5 3.7 %convolution_convert_fusion.1 = bf16[1024,256]{1,0:T(8,128)(2,1)S(1)} fusion(bf16[1024,2048]{1,0:T(8,128)(2,1)} %fusion.2, bf16[2048,256]{1,0:T(8,128)(2,1)} %all-gather.12.cloned.1.call-done), kind=kOutput, calls=%fused_computation.24 | convolution fusion | flops 1074003968 | bytes 5767168 | tf_op jit(solution)/shard_map/dot_general | solution.py:79
  56.2 2.5 collective-permute-start.1
  58.7 34.9 %all-gather.10.cloned.1.call-done = bf16[2048,256]{1,0:T(8,128)(2,1)} async-done(((bf16[256,256]{1,0:T(8,128)(2,1)}), bf16[2048,256]{1,0:T(8,128)(2,1)}) %all-gather.10.cloned.1.call-update) | async-done | bytes 1048592 | tf_op jit(solution)/shard_map/all_gather | solution.py:74
  93.6 3.7 %fusion.11 = f32[1024,256]{1,0:T(8,128)S(1)} fusion(bf16[1024,2048]{1,0:T(8,128)(2,1)} %fusion.2, bf16[2048,256]{1,0:T(8,128)(2,1)} %all-gather.10.cloned.1.call-done), kind=kOutput, calls=%fused_computation.22 | convolution fusion | flops 1074528256 | bytes 6291456 | tf_op jit(solution)/shard_map/dot_general | solution.py:79
  97.4 37.4 %all-gather.8.cloned.1.call-done = bf16[2048,256]{1,0:T(8,128)(2,1)} async-done(((bf16[256,256]{1,0:T(8,128)(2,1)}), bf16[2048,256]{1,0:T(8,128)(2,1)}) %all-gather.8.cloned.1.call-update) | async-done | bytes 1048592 | tf_op jit(solution)/shard_map/all_gather | solution.py:73
  134.8 3.7 %fusion.12 = bf16[1024,256]{1,0:T(8,128)(2,1)S(1)} fusion(f32[1024,256]{1,0:T(8,128)S(1)} %fusion.11, bf16[1024,2048]{1,0:T(8,128)(2,1)} %fusion.2, bf16[2048,256]{1,0:T(8,128)(2,1)} %all-gather.8.cloned.1.call-done), kind=kOutput, calls=%fused_computation.23 | convolution fusion | flops 1074266112 | bytes 6815744 | tf_op jit(solution)/shard_map/dot_general | solution.py:79
  139.2 3.1 collective-permute-start
  143.6 1.3 copy.38
  145.4 1.3 copy.40
  146.7 3.1 convert_multiply_fusion.2
  149.8 2.1 slice.587
  151.9 2.1 slice.588
  153.9 2.1 slice.586
  156.0 2.1 slice.590
  158.1 1.6 multiply_add_fusion.2
  159.7 1.4 slice.593
  161.1 1.4 slice.594
  162.4 1.4 slice.592
  163.8 1.4 slice.596
  165.2 2.0 multiply_add_fusion.3
  168.5 1.6 slice.598
  170.1 1.6 slice.602
  171.7 1.8 multiply_add_fusion.4
  173.5 1.5 slice.605
  175.1 1.5 slice.606
  176.6 1.5 slice.604
  178.1 1.5 slice.608
  183.1 1.5 multiply_add_fusion.6
  184.5 1.4 slice.617
  185.9 1.4 slice.618
  187.3 1.4 slice.616
  188.6 1.4 slice.620
  190.0 1.4 multiply_add_fusion.7
  192.6 1.3 slice.622
  193.9 1.3 slice.626
  195.2 1.3 multiply_add_fusion.8
  197.8 1.3 slice.630
  201.7 1.3 multiply_add_fusion.9
  208.1 1.3 slice.627
  213.2 1.3 slice.621
  217.8 1.4 slice.648
  225.0 1.5 slice.652
  229.0 1.6 slice.597
  233.6 1.4 slice.656
  236.1 2.1 slice.585
  238.1 2.1 slice.658
  252.7 2.7 pad.141
  255.7 1.4 fusion.61
  257.2 2.8 pad.140
  260.6 17.7 %all-gather.1 = f32[8,1,256]{2,1,0:T(1,128)S(1)} all-gather(f32[1,1,256]{2,1,0:T(1,128)S(1)} %add_bitcast_fusion), channel_id=1, replica_groups=mesh['sp'=8,'tp'=4] {'sp'}, dimensions={0}, use_global_device_ids=true | all-gather | bytes 9216 | tf_op jit(solution)/shard_map/all_gather | solution.py:22
  278.3 2.7 pad.161
  281.9 18.1 %all-gather = f32[8,1,256]{2,1,0:T(1,128)S(1)} all-gather(f32[1,1,256]{2,1,0:T(1,128)S(1)} %add_bitcast_fusion.1), channel_id=1, replica_groups=mesh['sp'=8,'tp'=4] {'sp'}, dimensions={0}, use_global_device_ids=true | all-gather | bytes 9216 | tf_op jit(solution)/shard_map/all_gather | solution.py:22
  300.4 4.6 %fusion.21 = bf16[1024,256]{1,0:T(8,128)(2,1)S(1)} fusion(f32[1024,256]{1,0:T(8,128)S(1)} %pad.160, f32[1024,256]{1,0:T(8,128)} %pad.161, f32[1024,256]{1,0:T(8,128)} %pad.140, f32[1024,256]{1,0:T(8,128)S(1)} %copy-done.2, f32[256]{0:T(256)S(1)} %get-tuple-element.49, bf16[1024,2048]{1,0:T(8,128)(2,1)} %fusion.2, ...), kind=kOutput, calls=%fused_computation.33 | convolution fusion | flops 1077411840 | bytes 9962496 | tf_op jit(solution)/shard_map/dot_general | solution.py:79
  306.0 4.3 %all-to-all-start.1 = ((bf16[4,256,256]{1,2,0:T(8,128)(2,1)}), bf16[4,256,256]{1,2,0:T(8,128)(2,1)}, u32[]{:S(2)}, u32[]{:S(2)}) async-start(bf16[4,256,256]{1,2,0:T(8,128)(2,1)} %copy.41), calls=%async_computation.1 | async-start | bytes 1048576 | tf_op jit(solution)/shard_map/all_to_all | solution.py:123
  311.5 4.0 %fusion.26 = f32[1024,256]{1,0:T(8,128)S(1)} fusion(f32[1054,256]{1,0:T(8,128)S(1)} %maximum_convert_fusion, f32[256]{0:T(256)S(1)} %bitcast.161, f32[256]{0:T(256)S(1)} %bitcast.159, f32[256]{0:T(256)S(1)} %bitcast.157, f32[256]{0:T(256)S(1)} %bitcast.155, f32[256]{0:T(256)S(1)} %bitcast.153, f32[256]{0:T(256)S(1)} %bitcast.151, f32[256]{0:T(256)S(1)} %bitcast.149, ...), kind=kLoop, calls=%fused_computation.43 | loop fusion | flops 15990784 | bytes 33586176 | tf_op jit(solution)/shard_map/add | solution.py:40
  317.8 1.6 copy.33
  319.3 5.1 %multiply_convert_fusion = bf16[1024,256]{1,0:T(8,128)(2,1)} fusion(f32[1024,256]{1,0:T(8,128)S(1)} %copy.34, f32[1024,256]{1,0:T(8,128)S(1)} %copy.33, f32[256]{0:T(256)S(1)} %copy-done.52, f32[1054,256]{1,0:T(8,128)S(1)} %maximum_convert_fusion, f32[256]{0:T(256)S(1)} %bitcast.162, f32[256]{0:T(256)S(1)} %bitcast.160, f32[256]{0:T(256)S(1)} %bitcast.158, ...), kind=kLoop, calls=%fused_computation.113 | loop fusion | flops 18087936 | bytes 35160064 | tf_op jit(solution)/shard_map/convert_element_type | solution.py:94
  325.7 11.6 %all_to_all.38 = bf16[4,256,256]{1,2,0:T(8,128)(2,1)S(1)} all-to-all(bf16[4,256,256]{1,2,0:T(8,128)(2,1)S(1)} %copy.35), channel_id=1, replica_groups=mesh['sp'=8,'tp'=4] {'tp'}, dimensions={0} | all-to-all | bytes 1048576 | tf_op jit(solution)/shard_map/all_to_all | solution.py:122
  337.3 6.9 %convolution_convert_fusion = bf16[256,2048]{1,0:T(8,128)(2,1)} fusion(bf16[2048,2048]{1,0:T(8,128)(2,1)} %all-gather.16.cloned.1.call-done, bf16[256,1024]{0,1:T(8,128)(2,1)} %bitcast.52, bf16[256,1024]{0,1:T(8,128)(2,1)S(1)} %bitcast.94), kind=kOutput, calls=%fused_computation.8 | convolution fusion | flops 2150105088 | bytes 10485760 | tf_op jit(solution)/shard_map/dot_general | solution.py:131
  (276 shorter events, 61.8 us)
Async XLA Ops:
  6.5 136.5 %copy-start = (bf16[4,64,64]{2,1,0:T(8,128)(2,1)S(1)}, bf16[4,64,64]{2,1,0:T(8,128)(2,1)}, u32[]{:S(2)}) copy-start(bf16[4,64,64]{2,1,0:T(8,128)(2,1)} %param.26) | copy-start | bytes 98308
  6.5 20.4 %copy-start.9 = (bf16[31,256]{1,0:T(8,128)(2,1)S(1)}, bf16[31,256]{1,0:T(8,128)(2,1)}, u32[]{:S(2)}) copy-start(bf16[31,256]{1,0:T(8,128)(2,1)} %param.23) | copy-start | bytes 47620
  6.5 45.9 %all-gather.12.cloned.1.call-start = ((), (), s32[]{:S(2)}) async-start(), calls=%async_computation.4 | async-start | bytes 1179648 | tf_op jit(solution)/shard_map/all_gather | solution.py:75
  7.3 86.3 %all-gather.10.cloned.1.call-start = ((), (), s32[]{:S(2)}) async-start(), calls=%async_computation.3 | async-start | bytes 1179648 | tf_op jit(solution)/shard_map/all_gather | solution.py:74
  8.0 126.7 %all-gather.8.cloned.1.call-start = ((), (), s32[]{:S(2)}) async-start(), calls=%async_computation.2 | async-start | bytes 1179648 | tf_op jit(solution)/shard_map/all_gather | solution.py:73
  8.7 291.3 %all-gather.14.cloned.1.call-start = ((), (), s32[]{:S(2)}) async-start(), calls=%async_computation.5 | async-start | bytes 1179648 | tf_op jit(solution)/shard_map/all_gather | solution.py:76
  9.3 328.0 %all-gather.16.cloned.1.call-start = ((), (), s32[]{:S(2)}) async-start(), calls=%async_computation.6 | async-start | bytes 9437184 | tf_op jit(solution)/shard_map/all_gather | solution.py:133
  18.2 13.1 %copy-start.51 = (bf16[2048]{0:T(1024)(128)(2,1)S(1)}, bf16[2048]{0:T(1024)(128)(2,1)}, u32[]{:S(2)}) copy-start(bf16[2048]{0:T(1024)(128)(2,1)} %param.18) | copy-start | bytes 12292
  18.2 13.2 %copy-start.55 = (bf16[256]{0:T(256)(128)(2,1)S(1)}, bf16[256]{0:T(256)(128)(2,1)}, u32[]{:S(2)}) copy-start(bf16[256]{0:T(256)(128)(2,1)} %param.24) | copy-start | bytes 1540
  18.2 13.7 %copy-start.43 = (bf16[4,256]{1,0:T(4,128)(2,1)S(1)}, bf16[4,256]{1,0:T(4,128)(2,1)}, u32[]{:S(2)}) copy-start(bf16[4,256]{1,0:T(4,128)(2,1)} %param.25) | copy-start | bytes 6148
  18.2 13.8 %copy-start.53 = (f32[256]{0:T(256)S(1)}, f32[256]{0:T(256)}, u32[]{:S(2)}) copy-start(f32[256]{0:T(256)} %param.28) | copy-start | bytes 3076
  56.2 86.0 %collective-permute-start.1 = (bf16[3,256]{1,0:T(4,128)(2,1)S(1)}, bf16[3,256]{1,0:T(4,128)(2,1)S(1)}, u32[]{:S(2)}, u32[]{:S(2)}) collective-permute-start(bf16[3,256]{1,0:T(4,128)(2,1)S(1)} %slice.744), channel_id=1, source_target_pairs={{0,4},{4,8},{8,12},{12,16},{16,20},{20,24},{24,28},{1,5},{5,9},{9,... | collective-permute-start | bytes 4616 | tf_op jit(solution)/shard_map/ppermute | solution.py:17
  138.5 3.8 %copy-start.4 = (bf16[1024,256]{1,0:T(8,128)(2,1)}, bf16[1024,256]{1,0:T(8,128)(2,1)S(1)}, u32[]{:S(2)}) copy-start(bf16[1024,256]{1,0:T(8,128)(2,1)S(1)} %fusion.12) | copy-start | bytes 1572868
  139.2 171.2 %collective-permute-start = (bf16[30,256]{1,0:T(8,128)(2,1)}, bf16[30,256]{1,0:T(8,128)(2,1)}, u32[]{:S(2)}, u32[]{:S(2)}) collective-permute-start(bf16[30,256]{1,0:T(8,128)(2,1)} %slice.681), channel_id=1, source_target_pairs={{0,4},{4,8},{8,12},{12,16},{16,20},{20,24},{24,28},{1,5},{5,9},{9,... | collective-permute-start | bytes 46088 | tf_op jit(solution)/shard_map/ppermute | solution.py:17
  142.8 2.1 copy-start.54
  224.1 21.0 %copy-start.10 = (f32[7,256]{1,0:T(8,128)S(1)}, f32[7,256]{1,0:T(8,128)}, u32[]{:S(2)}) copy-start(f32[7,256]{1,0:T(8,128)} %slice.621) | copy-start | bytes 21508
  224.1 21.0 %copy-start.11 = (f32[7,256]{1,0:T(8,128)S(1)}, f32[7,256]{1,0:T(8,128)}, u32[]{:S(2)}) copy-start(f32[7,256]{1,0:T(8,128)} %slice.646) | copy-start | bytes 21508
  235.5 15.5 %copy-start.8 = (f32[63,256]{1,0:T(8,128)S(1)}, f32[63,256]{1,0:T(8,128)}, u32[]{:S(2)}) copy-start(f32[63,256]{1,0:T(8,128)} %slice.652) | copy-start | bytes 193540
  235.5 15.7 %copy-start.6 = (f32[127,256]{1,0:T(8,128)S(1)}, f32[127,256]{1,0:T(8,128)}, u32[]{:S(2)}) copy-start(f32[127,256]{1,0:T(8,128)} %slice.597) | copy-start | bytes 390148
  235.5 15.7 %copy-start.7 = (f32[127,256]{1,0:T(8,128)S(1)}, f32[127,256]{1,0:T(8,128)}, u32[]{:S(2)}) copy-start(f32[127,256]{1,0:T(8,128)} %slice.654) | copy-start | bytes 390148
  236.0 15.0 %copy-start.50 = (f32[1,256]{1,0:T(1,128)S(1)}, f32[1,256]{1,0:T(1,128)}, u32[]{:S(2)}) copy-start(f32[1,256]{1,0:T(1,128)} %slice.787) | copy-start | bytes 3076
  236.1 15.1 %copy-start.49 = (f32[1,256]{1,0:T(1,128)S(1)}, f32[1,256]{1,0:T(1,128)}, u32[]{:S(2)}) copy-start(f32[1,256]{1,0:T(1,128)} %slice.755) | copy-start | bytes 3076
  238.1 14.0 %copy-start.48 = (f32[1,256]{1,0:T(1,128)S(1)}, f32[1,256]{1,0:T(1,128)}, u32[]{:S(2)}) copy-start(f32[1,256]{1,0:T(1,128)} %slice.754) | copy-start | bytes 3076
  248.7 3.6 %copy-start.3 = (f32[255,256]{1,0:T(8,128)S(1)}, f32[255,256]{1,0:T(8,128)}, u32[]{:S(2)}) copy-start(f32[255,256]{1,0:T(8,128)} %slice.656) | copy-start | bytes 783364
  251.1 1.3 copy-start.47
  252.2 3.2 copy-start.46
  255.4 1.7 copy-start.45
  255.7 25.4 %copy-start.44 = (f32[1,256]{1,0:T(1,128)S(1)}, f32[1,256]{1,0:T(1,128)}, u32[]{:S(2)}) copy-start(f32[1,256]{1,0:T(1,128)} %slice.784) | copy-start | bytes 3076
  257.1 43.0 %copy-start.2 = (f32[1024,256]{1,0:T(8,128)S(1)}, f32[1024,256]{1,0:T(8,128)}, u32[]{:S(2)}) copy-start(f32[1024,256]{1,0:T(8,128)} %pad.141) | copy-start | bytes 3145732
  300.1 10.3 %copy-start.5 = (bf16[1024,256]{1,0:T(8,128)(2,1)S(1)}, bf16[1024,256]{1,0:T(8,128)(2,1)}, u32[]{:S(2)}) copy-start(bf16[1024,256]{1,0:T(8,128)(2,1)} %copy-done.4) | copy-start | bytes 1572868
  300.1 11.1 %copy-start.12 = (f32[1,256]{1,0:T(1,128)S(1)}, f32[1,256]{1,0:T(1,128)}, u32[]{:S(2)}) copy-start(f32[1,256]{1,0:T(1,128)} %get-tuple-element.84) | copy-start | bytes 3076
  300.1 11.1 %copy-start.13 = (f32[1,256]{1,0:T(1,128)S(1)}, f32[1,256]{1,0:T(1,128)}, u32[]{:S(2)}) copy-start(f32[1,256]{1,0:T(1,128)} %get-tuple-element.85) | copy-start | bytes 3076
  300.1 11.1 %copy-start.14 = (f32[1,256]{1,0:T(1,128)S(1)}, f32[1,256]{1,0:T(1,128)}, u32[]{:S(2)}) copy-start(f32[1,256]{1,0:T(1,128)} %get-tuple-element.86) | copy-start | bytes 3076
  300.1 11.1 %copy-start.15 = (f32[1,256]{1,0:T(1,128)S(1)}, f32[1,256]{1,0:T(1,128)}, u32[]{:S(2)}) copy-start(f32[1,256]{1,0:T(1,128)} %get-tuple-element.87) | copy-start | bytes 3076
  300.1 11.1 %copy-start.16 = (f32[1,256]{1,0:T(1,128)S(1)}, f32[1,256]{1,0:T(1,128)}, u32[]{:S(2)}) copy-start(f32[1,256]{1,0:T(1,128)} %get-tuple-element.88) | copy-start | bytes 3076
  300.1 11.1 %copy-start.17 = (f32[1,256]{1,0:T(1,128)S(1)}, f32[1,256]{1,0:T(1,128)}, u32[]{:S(2)}) copy-start(f32[1,256]{1,0:T(1,128)} %get-tuple-element.89) | copy-start | bytes 3076
  300.1 11.1 %copy-start.18 = (f32[1,256]{1,0:T(1,128)S(1)}, f32[1,256]{1,0:T(1,128)}, u32[]{:S(2)}) copy-start(f32[1,256]{1,0:T(1,128)} %get-tuple-element.90) | copy-start | bytes 3076
  300.1 11.1 %copy-start.19 = (f32[1,256]{1,0:T(1,128)S(1)}, f32[1,256]{1,0:T(1,128)}, u32[]{:S(2)}) copy-start(f32[1,256]{1,0:T(1,128)} %get-tuple-element.91) | copy-start | bytes 3076
  300.1 11.1 %copy-start.20 = (f32[1,256]{1,0:T(1,128)S(1)}, f32[1,256]{1,0:T(1,128)}, u32[]{:S(2)}) copy-start(f32[1,256]{1,0:T(1,128)} %get-tuple-element.92) | copy-start | bytes 3076
  300.2 11.1 %copy-start.21 = (f32[1,256]{1,0:T(1,128)S(1)}, f32[1,256]{1,0:T(1,128)}, u32[]{:S(2)}) copy-start(f32[1,256]{1,0:T(1,128)} %get-tuple-element.93) | copy-start | bytes 3076
  300.2 11.1 %copy-start.22 = (f32[1,256]{1,0:T(1,128)S(1)}, f32[1,256]{1,0:T(1,128)}, u32[]{:S(2)}) copy-start(f32[1,256]{1,0:T(1,128)} %get-tuple-element.94) | copy-start | bytes 3076
  300.2 11.1 %copy-start.23 = (f32[1,256]{1,0:T(1,128)S(1)}, f32[1,256]{1,0:T(1,128)}, u32[]{:S(2)}) copy-start(f32[1,256]{1,0:T(1,128)} %get-tuple-element.95) | copy-start | bytes 3076
  300.2 11.1 %copy-start.24 = (f32[1,256]{1,0:T(1,128)S(1)}, f32[1,256]{1,0:T(1,128)}, u32[]{:S(2)}) copy-start(f32[1,256]{1,0:T(1,128)} %get-tuple-element.96) | copy-start | bytes 3076
  300.2 11.1 %copy-start.25 = (f32[1,256]{1,0:T(1,128)S(1)}, f32[1,256]{1,0:T(1,128)}, u32[]{:S(2)}) copy-start(f32[1,256]{1,0:T(1,128)} %get-tuple-element.97) | copy-start | bytes 3076
  300.2 11.1 %copy-start.26 = (f32[1,256]{1,0:T(1,128)S(1)}, f32[1,256]{1,0:T(1,128)}, u32[]{:S(2)}) copy-start(f32[1,256]{1,0:T(1,128)} %get-tuple-element.98) | copy-start | bytes 3076
  300.2 11.1 %copy-start.27 = (f32[1,256]{1,0:T(1,128)S(1)}, f32[1,256]{1,0:T(1,128)}, u32[]{:S(2)}) copy-start(f32[1,256]{1,0:T(1,128)} %get-tuple-element.99) | copy-start | bytes 3076
  300.2 11.1 %copy-start.28 = (f32[1,256]{1,0:T(1,128)S(1)}, f32[1,256]{1,0:T(1,128)}, u32[]{:S(2)}) copy-start(f32[1,256]{1,0:T(1,128)} %get-tuple-element.100) | copy-start | bytes 3076
  300.2 11.1 %copy-start.29 = (f32[1,256]{1,0:T(1,128)S(1)}, f32[1,256]{1,0:T(1,128)}, u32[]{:S(2)}) copy-start(f32[1,256]{1,0:T(1,128)} %get-tuple-element.101) | copy-start | bytes 3076
  300.2 11.1 %copy-start.30 = (f32[1,256]{1,0:T(1,128)S(1)}, f32[1,256]{1,0:T(1,128)}, u32[]{:S(2)}) copy-start(f32[1,256]{1,0:T(1,128)} %get-tuple-element.102) | copy-start | bytes 3076
  300.3 11.1 %copy-start.31 = (f32[1,256]{1,0:T(1,128)S(1)}, f32[1,256]{1,0:T(1,128)}, u32[]{:S(2)}) copy-start(f32[1,256]{1,0:T(1,128)} %get-tuple-element.103) | copy-start | bytes 3076
  300.3 11.1 %copy-start.32 = (f32[1,256]{1,0:T(1,128)S(1)}, f32[1,256]{1,0:T(1,128)}, u32[]{:S(2)}) copy-start(f32[1,256]{1,0:T(1,128)} %get-tuple-element.104) | copy-start | bytes 3076
  300.3 11.1 %copy-start.33 = (f32[1,256]{1,0:T(1,128)S(1)}, f32[1,256]{1,0:T(1,128)}, u32[]{:S(2)}) copy-start(f32[1,256]{1,0:T(1,128)} %get-tuple-element.105) | copy-start | bytes 3076
  300.3 11.1 %copy-start.34 = (f32[1,256]{1,0:T(1,128)S(1)}, f32[1,256]{1,0:T(1,128)}, u32[]{:S(2)}) copy-start(f32[1,256]{1,0:T(1,128)} %get-tuple-element.106) | copy-start | bytes 3076
  300.3 11.1 %copy-start.35 = (f32[1,256]{1,0:T(1,128)S(1)}, f32[1,256]{1,0:T(1,128)}, u32[]{:S(2)}) copy-start(f32[1,256]{1,0:T(1,128)} %get-tuple-element.107) | copy-start | bytes 3076
  300.3 11.1 %copy-start.36 = (f32[1,256]{1,0:T(1,128)S(1)}, f32[1,256]{1,0:T(1,128)}, u32[]{:S(2)}) copy-start(f32[1,256]{1,0:T(1,128)} %get-tuple-element.108) | copy-start | bytes 3076
  300.3 11.1 %copy-start.37 = (f32[1,256]{1,0:T(1,128)S(1)}, f32[1,256]{1,0:T(1,128)}, u32[]{:S(2)}) copy-start(f32[1,256]{1,0:T(1,128)} %get-tuple-element.109) | copy-start | bytes 3076
  300.3 11.1 %copy-start.38 = (f32[1,256]{1,0:T(1,128)S(1)}, f32[1,256]{1,0:T(1,128)}, u32[]{:S(2)}) copy-start(f32[1,256]{1,0:T(1,128)} %get-tuple-element.110) | copy-start | bytes 3076
  300.3 11.1 %copy-start.39 = (f32[1,256]{1,0:T(1,128)S(1)}, f32[1,256]{1,0:T(1,128)}, u32[]{:S(2)}) copy-start(f32[1,256]{1,0:T(1,128)} %get-tuple-element.111) | copy-start | bytes 3076
  300.3 11.1 %copy-start.40 = (f32[1,256]{1,0:T(1,128)S(1)}, f32[1,256]{1,0:T(1,128)}, u32[]{:S(2)}) copy-start(f32[1,256]{1,0:T(1,128)} %get-tuple-element.112) | copy-start | bytes 3076
  300.4 11.1 %copy-start.41 = (f32[1,256]{1,0:T(1,128)S(1)}, f32[1,256]{1,0:T(1,128)}, u32[]{:S(2)}) copy-start(f32[1,256]{1,0:T(1,128)} %get-tuple-element.113) | copy-start | bytes 3076
  300.4 11.1 %copy-start.42 = (f32[1,256]{1,0:T(1,128)S(1)}, f32[1,256]{1,0:T(1,128)}, u32[]{:S(2)}) copy-start(f32[1,256]{1,0:T(1,128)} %get-tuple-element.114) | copy-start | bytes 3076
  306.0 19.7 %all-to-all-start.1 = ((bf16[4,256,256]{1,2,0:T(8,128)(2,1)}), bf16[4,256,256]{1,2,0:T(8,128)(2,1)}, u32[]{:S(2)}, u32[]{:S(2)}) async-start(bf16[4,256,256]{1,2,0:T(8,128)(2,1)} %copy.41), calls=%async_computation.1 | async-start | bytes 1048576 | tf_op jit(solution)/shard_map/all_to_all | solution.py:123
  315.9 3.4 copy-start.52
  337.3 6.9 %copy-start.1 = (bf16[4,64,64]{2,1,0:T(8,128)(2,1)S(1)}, bf16[4,64,64]{2,1,0:T(8,128)(2,1)}, u32[]{:S(2)}) copy-start(bf16[4,64,64]{2,1,0:T(8,128)(2,1)} %param.26) | copy-start | bytes 98308
Sparse Core Ops, SparseCore 0:
  9.5 42.9 all-gather.11
  54.6 38.9 all-gather.9
  95.7 38.9 all-gather.7
  136.7 38.9 all-gather.13
  177.7 123.8 all-gather.15
where the time goes:
time: 353 us; the launch traced here: 351 us
  local copies, waits for them, and re-layouts  99.4 us (28%)
  waiting for transfers between devices  90.1 us (26%)
  blocking collectives  63.9 us (18%)
  other arithmetic  49.1 us (14%)
  matrix products  23.8 us (7%)
  between operations  14.5 us (4%)
  starting transfers between devices  10 us (3%)
    slice x68, local copies, waits for them, and re-layouts, body(): lax.associative_scan(merge_pair, (decay, drive), axis=0)  79.6 us
    all_gather x1, waiting for transfers between devices, body(): lax.all_gather(value_proj, 'sp', axis=0, tiled=True)  37.4 us
    all_gather x2, blocking collectives, prefix(): gathered = jax.tree.map(lambda a: lax.all_gather(a, axis), part)  35.8 us
    all_gather x1, waiting for transfers between devices, body(): lax.all_gather(glu_proj, 'sp', axis=0, tiled=True)  34.9 us
    add x17, other arithmetic, merge_pair(): return (earlier[0] * later[0], later[0] * earlier[1] + later[1])  16.4 us
    dot_general x4, matrix products, body(): jnp.dot(normed, piece, preferred_element_type=f32)  15.9 us
    all_gather x1, waiting for transfers between devices, body(): lax.all_gather(recur_proj, 'sp', axis=0, tiled=True)  15.1 us
    all_to_all x1, blocking collectives, body(): lax.all_to_all(y_conv, 'tp', split_axis=0, concat_axis=1, tiled=True)  11.6 us
  transfers between devices with their start and end apart: 8, of which 3 were waited for; matrix products, arithmetic and copies ran while one was open for 47% of the time, Pallas kernels for 0%

commit v1 on v0

v1 whole, which is shorter than its diff:
```python
import functools

import jax
import jax.numpy as jnp
from jax import lax
from jax.experimental import pallas as pl
from jax.experimental.pallas import tpu as pltpu
from jax.sharding import PartitionSpec as P

GROUP_CH = 64
HEAD_CH = 64
HALO = 32

eps = 1e-06
gate_scale = 8.0
f32 = jnp.float32
bf16 = jnp.bfloat16


def vmem():
    return pl.BlockSpec(memory_space=pltpu.VMEM)


def project_kernel(x_ref, gain_ref, w_ref, g_ref, r_ref, b_ref):
    x = x_ref[...].astype(f32)
    scale = lax.rsqrt(jnp.mean(x * x, axis=-1, keepdims=True) + eps)
    normed = (x * scale * gain_ref[...]).astype(bf16)
    c = g_ref.shape[1]

    def part(i):
        return jnp.dot(normed, w_ref[:, i * c : (i + 1) * c], preferred_element_type=f32)

    g_ref[...] = (part(0) * jax.nn.sigmoid(part(1))).astype(bf16).astype(f32)
    r_ref[...] = part(2).astype(bf16).astype(f32)
    b_ref[...] = jax.nn.gelu(part(3), approximate=True)


def project(tokens, gain, w, tile=256):
    rows, d = tokens.shape
    c = w.shape[1] // 4
    out = jax.ShapeDtypeStruct((rows, c), f32)
    spec = pl.BlockSpec((tile, c), lambda i: (i, 0))
    return pl.pallas_call(
        project_kernel,
        grid=(rows // tile,),
        in_specs=[
            pl.BlockSpec((tile, d), lambda i: (i, 0)),
            pl.BlockSpec((1, d), lambda i: (0, 0)),
            pl.BlockSpec(w.shape, lambda i: (0, 0)),
        ],
        out_specs=[spec] * 3,
        out_shape=[out] * 3,
        cost_estimate=pl.CostEstimate(
            flops=2 * rows * d * 4 * c, bytes_accessed=12 * 2**20, transcendentals=2 * rows * c
        ),
        name="project",
    )(tokens, gain, w)


def split_dot(x, m):
    hi = x.astype(bf16)
    rest = x - hi.astype(f32)
    mid = rest.astype(bf16)
    low = (rest - mid.astype(f32)).astype(bf16)
    dot = functools.partial(jnp.dot, preferred_element_type=f32)
    return dot(hi, m) + dot(mid, m) + dot(low, m)


def window_sum(window, taps_ref, cols, length):
    taps = taps_ref.shape[0]
    total = jnp.zeros((length, window.shape[1]), f32)
    for shift in range(8):
        offsets = [k for k in range(taps) if (HALO - taps + 1 + k) % 8 == shift]
        if not offsets:
            continue
        moved = pltpu.roll(window, window.shape[0] - shift, 0) if shift else window
        for k in offsets:
            at = HALO - taps + 1 + k - shift
            total = total + taps_ref[k : k + 1, cols] * moved[at : at + length]
    return total


def mixers_kernel(
    tile,
    g_ref,
    gh_ref,
    r_ref,
    rh_ref,
    ed_ref,
    taps_ref,
    gain_ref,
    short_ref,
    maps_ref,
    rate_ref,
    yc_ref,
    s_ref,
    a_ref,
    last_ref,
    gbuf,
    rbuf,
    cbuf,
):
    rows, c = g_ref.shape
    taps = taps_ref.shape[0]
    shorts = short_ref.shape[0]
    gbuf[0:HALO] = gh_ref[...]
    rbuf[0:HALO] = rh_ref[...]
    gbuf[HALO:] = g_ref[...]
    rbuf[HALO:] = r_ref[...]
    row_group = lax.broadcasted_iota(jnp.int32, (c, c), 0) // GROUP_CH
    col_group = lax.broadcasted_iota(jnp.int32, (c, c), 1) // GROUP_CH
    mean_map = jnp.where(row_group == col_group, 1.0 / GROUP_CH, 0.0).astype(bf16)
    sub = lax.broadcasted_iota(jnp.int32, (tile // 8, 8, c), 1)

    def step(i, carry):
        decay_in, state_in = carry
        t0 = pl.multiple_of(i * tile, tile)
        for lane in range(0, c, 128):
            cols = slice(lane, lane + 128)
            for part in range(0, tile, 64):
                cbuf[part : part + 64, cols] = window_sum(
                    gbuf[pl.ds(t0 + part, 64 + HALO), cols], taps_ref, cols, 64
                )
        x = cbuf[...]
        spread = x - split_dot(x, mean_map)
        var = split_dot(spread * spread, mean_map)
        yc_ref[pl.ds(t0, tile), :] = jax.nn.silu(
            spread * lax.rsqrt(var + eps) * gain_ref[...]
        ).astype(bf16)
        rc = window_sum(rbuf[pl.ds(t0, tile + HALO), :], short_ref, slice(None), tile)
        rc = rc.astype(bf16)
        gates = jax.nn.sigmoid(jnp.dot(rc, maps_ref[...], preferred_element_type=f32))
        log_decay = -gate_scale * gates[:, :c] * rate_ref[...] + ed_ref[pl.ds(t0, tile), :]
        y = 2.0 * log_decay
        series = jnp.full_like(y, 1.0 / 3628800.0)
        for inv in (362880.0, 40320.0, 5040.0, 720.0, 120.0, 24.0, 6.0, 2.0, 1.0):
            series = series * y + 1.0 / inv
        one_minus = jnp.where(y > -0.5, -y * series, 1.0 - jnp.exp(y))
        b = jnp.sqrt(one_minus) * gates[:, c:] * rc.astype(f32)
        a = jnp.exp(log_decay)
        a = a.reshape(tile // 8, 8, c)
        b = b.reshape(tile // 8, 8, c)
        for shift in (1, 2, 4):
            keep = sub >= shift
            a_prev = jnp.where(keep, pltpu.roll(a, shift, 1), 1.0)
            b_prev = jnp.where(keep, pltpu.roll(b, shift, 1), 0.0)
            b = b + a * b_prev
            a = a * a_prev
        for n in range(tile // 8):
            state = b[n] + a[n] * state_in
            decay = a[n] * decay_in
            s_ref[pl.ds(t0 + 8 * n, 8), :] = state
            a_ref[pl.ds(t0 + 8 * n, 8), :] = decay
            state_in = state[7:8]
            decay_in = decay[7:8]
        return decay_in, state_in

    decay, state = lax.fori_loop(
        0, rows // tile, step, (jnp.ones((1, c), f32), jnp.zeros((1, c), f32))
    )
    last_ref[0:1] = decay
    last_ref[1:2] = state


def mixers(gated, gh, rec, rh, extra, taps, gain, short, maps, rate, tile=128):
    rows, c = gated.shape
    big = jax.ShapeDtypeStruct((rows, c), f32)
    return pl.pallas_call(
        functools.partial(mixers_kernel, tile),
        in_specs=[vmem()] * 10,
        out_specs=[vmem()] * 4,
        out_shape=[
            jax.ShapeDtypeStruct((rows, c), bf16),
            big,
            big,
            jax.ShapeDtypeStruct((2, c), f32),
        ],
        scratch_shapes=[
            pltpu.VMEM((HALO + rows, c), f32),
            pltpu.VMEM((HALO + rows, c), f32),
            pltpu.VMEM((tile, c), f32),
        ],
        cost_estimate=pl.CostEstimate(
            flops=200 * rows * c * 60, bytes_accessed=8 * 2**20, transcendentals=8 * rows * c
        ),
        name="mixers",
    )(gated, gh, rec, rh, extra, taps, gain, short, maps, rate)


def output_kernel(y_ref, w_ref, o_ref):
    k = y_ref.shape[1]
    o_ref[...] = jnp.dot(
        y_ref[...], w_ref[...].reshape(k, w_ref.shape[-1]), preferred_element_type=f32
    ).astype(bf16)


def output(y, w):
    rows, k = y.shape
    sp, tp, part, cols = w.shape
    if cols % 128:
        full = jnp.transpose(w, (1, 2, 0, 3)).reshape(tp * part, sp * cols)
        return jnp.dot(y, full, preferred_element_type=f32).astype(bf16)
    return pl.pallas_call(
        output_kernel,
        grid=(sp,),
        in_specs=[
            pl.BlockSpec((rows, k), lambda j: (0, 0)),
            pl.BlockSpec((None, tp, part, cols), lambda j: (j, 0, 0, 0)),
        ],
        out_specs=pl.BlockSpec((rows, cols), lambda j: (0, j)),
        out_shape=jax.ShapeDtypeStruct((rows, sp * cols), bf16),
        name="output",
    )(y, w)


def block_diagonal(blocks):
    h, n, _ = blocks.shape
    eye = jnp.eye(h, dtype=blocks.dtype)
    return (blocks[:, :, None, :] * eye[:, None, :, None]).reshape(h * n, h * n)


def from_behind(value, axis):
    count = lax.axis_size(axis)
    return lax.ppermute(value, axis, [(s, s + 1) for s in range(count - 1)])


def body(
    tokens,
    norm_gain,
    value_proj,
    glu_proj,
    recur_proj,
    branch_proj,
    channelwise_filter_taps,
    group_gain,
    short_kernel,
    decay_map,
    entry_gate_matrix,
    rate_param,
    extra_decay,
    conv_out,
    recur_out,
):
    rows = tokens.shape[0]
    c = value_proj.shape[1]
    sp = lax.axis_size("sp")
    tp = lax.axis_size("tp")
    w_in = jnp.concatenate([value_proj, glu_proj, recur_proj, branch_proj], axis=1)
    w_in = lax.all_gather(w_in, "sp", axis=0, tiled=True)
    w_out = jnp.concatenate([conv_out, recur_out], axis=0)
    w_out = lax.all_gather(w_out, ("sp", "tp"), axis=0, tiled=False)
    w_out = w_out.reshape(sp, tp, 2 * c, conv_out.shape[1])
    gated, rec, branch = project(tokens, norm_gain.astype(f32)[None], w_in)
    tail = jnp.concatenate([gated[rows - HALO :], rec[rows - HALO :]], axis=1).astype(bf16)
    head = from_behind(tail, "sp").astype(f32)
    maps = jnp.concatenate([block_diagonal(decay_map), block_diagonal(entry_gate_matrix)], axis=1)
    y_conv, local_state, running, last = mixers(
        gated,
        head[:, :c],
        rec,
        head[:, c:],
        extra_decay,
        channelwise_filter_taps.astype(f32),
        group_gain.astype(f32)[None],
        short_kernel.astype(f32),
        maps,
        jax.nn.softplus(-rate_param)[None],
    )
    lasts = lax.all_gather(last, "sp")
    place = lax.axis_index("sp")
    incoming = jnp.zeros((c,), f32)
    for hop in range(sp - 1):
        after = lasts[hop, 0] * incoming + lasts[hop, 1]
        incoming = jnp.where(hop < place, after, incoming)
    state = local_state + running * incoming[None]
    y_lru = (state * branch).astype(bf16)
    y = jnp.concatenate([y_conv, y_lru], axis=1)
    y = lax.all_to_all(y, "tp", split_axis=0, concat_axis=1, tiled=True)
    return output(y, w_out)


def solution(mesh):
    in_specs = (
        P("sp", None),
        P(),
        P("sp", "tp"),
        P("sp", "tp"),
        P("sp", "tp"),
        P("sp", "tp"),
        P(None, "tp"),
        P("tp"),
        P(None, "tp"),
        P("tp", None, None),
        P("tp", None, None),
        P("tp"),
        P("sp", "tp"),
        P("tp", "sp"),
        P("tp", "sp"),
    )
    out_specs = P(("sp", "tp"), None)
    return jax.shard_map(body, mesh=mesh, in_specs=in_specs, out_specs=out_specs, check_vma=False)
```

time: 353 us -> 184 us (0.52)
  the two profiles are of different devices: /device:TPU:0 before, /device:TPU:5 now
where the time goes in v1:
time: 184 us; the launch traced here: 183 us
  waiting for transfers between devices  72.7 us (40%)
  blocking collectives  46.7 us (25%)
  Pallas kernels  30.6 us (17%)
  between operations  13.5 us (7%)
  other arithmetic  12.9 us (7%)
  local copies, waits for them, and re-layouts  3.79 us (2%)
  starting transfers between devices  3.25 us (2%)
    all_gather x1, waiting for transfers between devices, body(): w_in = lax.all_gather(w_in, 'sp', axis=0, tiled=True)  66.9 us
    all_to_all x1, blocking collectives, body(): y = lax.all_to_all(y, 'tp', split_axis=0, concat_axis=1, tiled=True)  24.5 us
    all_gather x1, blocking collectives, body(): lasts = lax.all_gather(last, 'sp')  22.2 us
    pallas_call x1, Pallas kernels, mixers(): pl.pallas_call(functools.partial(mixers_kernel, tile), in_specs=[vmem()]...  12.5 us
    pallas_call x1, Pallas kernels, project(): pl.pallas_call(project_kernel, grid=(rows // tile,), in_specs=[pl.BlockSp...  9.46 us
    pallas_call x1, Pallas kernels, output(): pl.pallas_call(output_kernel, grid=(sp,), in_specs=[pl.BlockSpec((rows, k...  8.64 us
    all_gather x1, waiting for transfers between devices, body(): w_out = lax.all_gather(w_out, ('sp', 'tp'), axis=0, tiled=False)  5.78 us
  transfers between devices with their start and end apart: 3, of which 2 were waited for; matrix products, arithmetic and copies ran while one was open for 8% of the time, Pallas kernels for 12%

profile of v1, /device:TPU:5, one launch (start us, length us, event | category | flops | bytes accessed | tf_op | source)
XLA Modules:
  0.0 183.4 jit_solution(14756493270745589272)
XLA Ops:
  6.5 0.0 all-gather.6.cloned.1.call-start
  6.5 2.0 %pad_maximum_fusion.1 = bf16[256,1024]{1,0:T(8,128)(2,1)} fusion(bf16[256,256]{1,0:T(8,128)(2,1)} %param.20, bf16[256,256]{1,0:T(8,128)(2,1)} %param.19, bf16[256,256]{1,0:T(8,128)(2,1)} %param.18, bf16[256,256]{1,0:T(8,128)(2,1)} %param.17), kind=kLoop, calls=%fused_computation.2 | loop fusion | flops 2097152 | bytes 1048576 | tf_op jit(solution)/shard_map/concatenate | solution.py:248
  8.5 0.0 all-gather.6.cloned.1.call-update
  8.5 0.0 all-gather.8.cloned.1.call-start
  8.6 1.7 pad_maximum_fusion.3
  10.3 0.0 all-gather.8.cloned.1.call-update
  10.3 1.3 broadcast_in_dim.24
  11.6 1.2 broadcast_multiply_fusion.1
  12.8 0.2 mul.101
  13.0 0.2 mul.98
  13.2 1.3 compare_select_fusion
  14.5 66.9 %all-gather.6.cloned.1.call-done.w_ref = bf16[2048,1024]{1,0:T(8,128)(2,1)} async-done(((bf16[256,1024]{1,0:T(8,128)(2,1)}), bf16[2048,1024]{1,0:T(8,128)(2,1)}) %all-gather.6.cloned.1.call-update) | async-done | bytes 4194320 | tf_op jit(solution)/shard_map/all_gather | solution.py:249
  81.4 0.0 copy-start.1
  81.4 0.0 copy-start.2
  81.4 0.0 copy-start.3
  81.4 9.5 %project.1 = (f32[1024,256]{1,0:T(8,128)}, f32[1024,256]{1,0:T(8,128)}, f32[1024,256]{1,0:T(8,128)}) custom-call(bf16[1024,2048]{1,0:T(8,128)(2,1)} %x_ref.1, f32[1,2048]{1,0:T(1,128)} %bitcast.26, bf16[2048,1024]{1,0:T(8,128)(2,1)} %all-gather.6.cloned.1.call-done.w_ref), custom_call_target="tpu_custom_call" | custom-call | flops 4294967296 | bytes 12582912 | tf_op jit(solution)/shard_map/project/pallas_call | solution.py:43
  90.8 0.8 slice.100
  91.6 0.8 slice.101
  92.4 3.2 %collective-permute-start = (bf16[32,512]{1,0:T(8,128)(2,1)S(1)}, bf16[32,512]{1,0:T(8,128)(2,1)S(1)}, u32[]{:S(2)}, u32[]{:S(2)}) collective-permute-start(bf16[32,512]{1,0:T(8,128)(2,1)S(1)} %pad_maximum_fusion.4), channel_id=1, source_target_pairs={{0,4},{4,8},{8,12},{12,16},{16,20},{20,24},{24,28},{1,5},{5,9},{9,... | collective-permute-start | bytes 98312 | tf_op jit(solution)/shard_map/ppermute | solution.py:224
  95.6 0.7 pad_maximum_fusion.2.maps_ref
  96.3 0.0 copy-done.1
  96.3 0.6 convert_element_type.26.taps_ref
  96.9 0.0 copy-done.2
  96.9 0.6 convert_element_type.27.short_ref
  97.5 0.0 copy-done.3
  97.5 0.6 broadcast_in_dim.25
  98.1 0.0 collective-permute-done
  98.1 0.6 fusion.1
  98.7 0.0 copy-start
  98.7 12.5 %mixers.1 = (bf16[1024,256]{1,0:T(8,128)(2,1)}, f32[1024,256]{1,0:T(8,128)}, f32[1024,256]{1,0:T(8,128)}, f32[2,256]{1,0:T(2,128)}) custom-call(f32[1024,256]{1,0:T(8,128)} %get-tuple-element.12.g_ref, f32[32,256]{1,0:T(8,128)} %get-tuple-element.20.gh_ref, f32[1024,256]{1,0:T(8,128)} %get-tuple-element.13.r_ref, f32[32,256]{1,0:T(8,128)} %get-tuple-element.19.rh_ref, ...), custom_call_target="tpu_custom_call" | custom-call | flops 3145728000 | bytes 8388608 | tf_op jit(solution)/shard_map/mixers/pallas_call | solution.py:168
  111.2 22.2 %all-gather.2 = f32[8,2,256]{2,1,0:T(2,128)S(1)} all-gather(f32[1,2,256]{2,1,0:T(2,128)} %bitcast.40), channel_id=2, replica_groups=mesh['sp'=8,'tp'=4] {'sp'}, dimensions={0}, use_global_device_ids=true | all-gather | bytes 18432 | tf_op jit(solution)/shard_map/all_gather | solution.py:269
  133.5 0.0 copy-done
  133.5 1.8 %multiply_convert_fusion = bf16[1024,256]{1,0:T(8,128)(2,1)S(1)} fusion(f32[1024,256]{1,0:T(8,128)S(1)} %copy-done, f32[1024,256]{1,0:T(8,128)} %get-tuple-element.15, f32[1024,256]{1,0:T(8,128)} %get-tuple-element.16, f32[256]{0:T(256)S(1)} %add_select_fusion), kind=kLoop, calls=%fused_computation.1 | loop fusion | flops 1048576 | bytes 3671040 | tf_op jit(solution)/shard_map/convert_element_type | solution.py:276
  135.3 1.1 pad_maximum_fusion
  136.4 24.5 %all_to_all.19 = bf16[4,256,512]{2,1,0:T(8,128)(2,1)S(1)} all-to-all(bf16[4,256,512]{2,1,0:T(8,128)(2,1)S(1)} %bitcast.24), channel_id=1, replica_groups=mesh['sp'=8,'tp'=4] {'tp'}, dimensions={0} | all-to-all | bytes 2097152 | tf_op jit(solution)/shard_map/all_to_all | solution.py:278
  160.9 1.2 copy.18
  162.1 5.8 %all-gather.8.cloned.1.call-done = bf16[16384,256]{1,0:T(8,128)(2,1)} async-done(((bf16[512,256]{1,0:T(8,128)(2,1)}), bf16[16384,256]{1,0:T(8,128)(2,1)}) %all-gather.8.cloned.1.call-update) | async-done | bytes 8388624 | tf_op jit(solution)/shard_map/all_gather | solution.py:251
  167.9 8.6 %output.1 = bf16[256,2048]{1,0:T(8,128)(2,1)} custom-call(bf16[256,2048]{1,0:T(8,128)(2,1)} %bitcast.23, bf16[8,4,512,256]{3,2,1,0:T(8,128)(2,1)} %bitcast.22), custom_call_target="tpu_custom_call" | custom-call | tf_op jit(solution)/shard_map/output/pallas_call | solution.py:203
  (4 shorter events, 0.0 us)
Async XLA Ops:
  6.5 74.8 %all-gather.6.cloned.1.call-start = ((), (), s32[]{:S(2)}) async-start(), calls=%async_computation.1 | async-start | bytes 4718592 | tf_op jit(solution)/shard_map/all_gather | solution.py:249
  8.5 159.4 %all-gather.8.cloned.1.call-start = ((), (), s32[]{:S(2)}) async-start(), calls=%async_computation.2 | async-start | bytes 8650752 | tf_op jit(solution)/shard_map/all_gather | solution.py:251
  81.4 14.9 %copy-start.1 = (bf16[31,256]{1,0:T(8,128)(2,1)S(1)}, bf16[31,256]{1,0:T(8,128)(2,1)}, u32[]{:S(2)}) copy-start(bf16[31,256]{1,0:T(8,128)(2,1)} %param.21) | copy-start | bytes 47620
  81.4 15.5 %copy-start.2 = (bf16[4,256]{1,0:T(4,128)(2,1)S(1)}, bf16[4,256]{1,0:T(4,128)(2,1)}, u32[]{:S(2)}) copy-start(bf16[4,256]{1,0:T(4,128)(2,1)} %param.23) | copy-start | bytes 6148
  81.4 16.1 %copy-start.3 = (bf16[256]{0:T(256)(128)(2,1)S(1)}, bf16[256]{0:T(256)(128)(2,1)}, u32[]{:S(2)}) copy-start(bf16[256]{0:T(256)(128)(2,1)} %param.22) | copy-start | bytes 1540
  92.4 5.7 %collective-permute-start = (bf16[32,512]{1,0:T(8,128)(2,1)S(1)}, bf16[32,512]{1,0:T(8,128)(2,1)S(1)}, u32[]{:S(2)}, u32[]{:S(2)}) collective-permute-start(bf16[32,512]{1,0:T(8,128)(2,1)S(1)} %pad_maximum_fusion.4), channel_id=1, source_target_pairs={{0,4},{4,8},{8,12},{12,16},{16,20},{20,24},{24,28},{1,5},{5,9},{9,... | collective-permute-start | bytes 98312 | tf_op jit(solution)/shard_map/ppermute | solution.py:224
  98.7 34.8 %copy-start = (f32[1024,256]{1,0:T(8,128)S(1)}, f32[1024,256]{1,0:T(8,128)}, u32[]{:S(2)}) copy-start(f32[1024,256]{1,0:T(8,128)} %get-tuple-element.18) | copy-start | bytes 3145732
Sparse Core Ops, SparseCore 0:
  9.5 71.8 all-gather.5
  84.2 83.6 all-gather.7

commit v2 on v1

--- a/solution.py
+++ b/solution.py
@@ -19,6 +19,153 @@
 
 def vmem():
     return pl.BlockSpec(memory_space=pltpu.VMEM)
+
+
+def gather_kernel(lines, width, *refs):
+    count = 4
+    parts, out = refs[:count], refs[count]
+    send_up, recv_up, send_down, recv_down, send_side, recv_side, local = refs[count + 1 :]
+    c = parts[0].shape[1]
+    me = lax.axis_index("sp")
+    z, y = me // width, me % width
+
+    def signal(target):
+        pl.semaphore_signal(
+            barrier, inc=1, device_id={"sp": target}, device_id_type=pl.DeviceIdType.MESH
+        )
+
+    barrier = pltpu.get_barrier_semaphore()
+    above, below = z < lines - 1, z > 0
+    for d in (1, lines - 1) if lines > 2 else range(1, lines):
+        signal((z + d) % lines * width + y)
+    for d in range(1, width):
+        signal(z * width + (y + d) % width)
+    greeted = min(lines - 1, 2) + width - 1
+    if greeted:
+        pl.semaphore_wait(barrier, greeted)
+
+    def spot(block, i):
+        return out.at[block, :, pl.ds(i * c, c)]
+
+    def remote(own, block, i, send_sem, recv_sem, target):
+        return pltpu.make_async_remote_copy(
+            src_ref=parts[i] if own else spot(block, i),
+            dst_ref=spot(block, i),
+            send_sem=send_sem,
+            recv_sem=recv_sem,
+            device_id={"sp": target},
+            device_id_type=pl.DeviceIdType.MESH,
+        )
+
+    def up(s, i):
+        return remote(
+            s == 0, me - s * width, i, send_up.at[s, i], recv_up.at[s, i], me + width
+        )
+
+    def down(s, i):
+        return remote(
+            s == 0, me + s * width, i, send_down.at[s, i], recv_down.at[s, i], me - width
+        )
+
+    def arriving_up(s, i):
+        return remote(
+            False, me - s * width, i, send_up.at[s - 1, i], recv_up.at[s - 1, i], me - width
+        )
+
+    def arriving_down(s, i):
+        return remote(
+            False, me + s * width, i, send_down.at[s - 1, i], recv_down.at[s - 1, i], me + width
+        )
+
+    def side(s, d, i):
+        slot = s + lines - 1
+        target = z * width + (y + d) % width
+        return remote(
+            s == 0, me + s * width, i, send_side.at[slot, d - 1, i], recv_side.at[slot, d - 1, i],
+            target,
+        )
+
+    def arriving_side(s, d, i):
+        slot = s + lines - 1
+        source = z * width + (y + width - d) % width
+        return remote(
+            False, source + s * width, i, send_side.at[slot, d - 1, i],
+            recv_side.at[slot, d - 1, i], source,
+        )
+
+    def all_sides(s, i, act):
+        for d in range(1, width):
+            act(side(s, d, i))
+
+    def start(copy):
+        copy.start()
+
+    for i in range(count):
+        pl.when(above)(lambda: up(0, i).start())
+        pl.when(below)(lambda: down(0, i).start())
+        all_sides(0, i, start)
+    own = [pltpu.make_async_copy(parts[i], spot(me, i), local.at[i]) for i in range(count)]
+    for copy in own:
+        copy.start()
+    for s in range(1, lines):
+        for i in range(count):
+
+            @pl.when(z - s >= 0)
+            def _():
+                arriving_up(s, i).wait_recv()
+                if s < lines - 1:
+                    pl.when(above)(lambda: up(s, i).start())
+                all_sides(-s, i, start)
+
+            @pl.when(z + s < lines)
+            def _():
+                arriving_down(s, i).wait_recv()
+                if s < lines - 1:
+                    pl.when(below)(lambda: down(s, i).start())
+                all_sides(s, i, start)
+
+    for copy in own:
+        copy.wait()
+    for s in range(1 - lines, lines):
+        for i in range(count):
+
+            @pl.when((z + s >= 0) & (z + s < lines))
+            def _():
+                for d in range(1, width):
+                    arriving_side(s, d, i).wait_recv()
+                    side(s, d, i).wait_send()
+
+    for s in range(lines - 1):
+        for i in range(count):
+            pl.when(above & (z - s >= 0))(lambda: up(s, i).wait_send())
+            pl.when(below & (z + s < lines))(lambda: down(s, i).wait_send())
+
+
+def gather_input(parts, lines, width):
+    k, c = parts[0].shape
+    dma = pltpu.SemaphoreType.DMA
+    steps = max(lines - 1, 1)
+    sides = (2 * lines - 1, max(width - 1, 1), 4)
+    return pl.pallas_call(
+        functools.partial(gather_kernel, lines, width),
+        in_specs=[vmem()] * 4,
+        out_specs=vmem(),
+        out_shape=jax.ShapeDtypeStruct((lines * width, k, 4 * c), bf16),
+        scratch_shapes=[
+            dma((steps, 4)),
+            dma((steps, 4)),
+            dma((steps, 4)),
+            dma((steps, 4)),
+            dma(sides),
+            dma(sides),
+            dma((4,)),
+        ],
+        compiler_params=pltpu.CompilerParams(collective_id=0, has_side_effects=True),
+        cost_estimate=pl.CostEstimate(
+            flops=0, bytes_accessed=128 * 2**20, transcendentals=0
+        ),
+        name="gather",
+    )(*parts)
 
 
 def project_kernel(x_ref, gain_ref, w_ref, g_ref, r_ref, b_ref):
@@ -245,11 +392,13 @@
     c = value_proj.shape[1]
     sp = lax.axis_size("sp")
     tp = lax.axis_size("tp")
-    w_in = jnp.concatenate([value_proj, glu_proj, recur_proj, branch_proj], axis=1)
-    w_in = lax.all_gather(w_in, "sp", axis=0, tiled=True)
+    width = max(tp // 2, 1)
+    width = width if sp % width == 0 else 1
     w_out = jnp.concatenate([conv_out, recur_out], axis=0)
     w_out = lax.all_gather(w_out, ("sp", "tp"), axis=0, tiled=False)
     w_out = w_out.reshape(sp, tp, 2 * c, conv_out.shape[1])
+    w_in = gather_input([value_proj, glu_proj, recur_proj, branch_proj], sp // width, width)
+    w_in = w_in.reshape(-1, 4 * c)
     gated, rec, branch = project(tokens, norm_gain.astype(f32)[None], w_in)
     tail = jnp.concatenate([gated[rows - HALO :], rec[rows - HALO :]], axis=1).astype(bf16)
     head = from_behind(tail, "sp").astype(f32)

time: 184 us -> 174 us (0.946)
  the two profiles are of different devices: /device:TPU:5 before, /device:TPU:0 now
where the time goes in v2:
time: 174 us; the launch traced here: 173 us
  Pallas kernels  101 us (58%)
  blocking collectives  43.2 us (25%)
  between operations  13.5 us (8%)
  other arithmetic  9.3 us (5%)
  local copies, waits for them, and re-layouts  3.82 us (2%)
  starting transfers between devices  2.56 us (1%)
    pallas_call x1, Pallas kernels, gather_input(): pl.pallas_call(functools.partial(gather_kernel, lines, width), in_specs=[...  70.2 us
    all_gather x1, blocking collectives, body(): lasts = lax.all_gather(last, 'sp')  26.3 us
    all_to_all x1, blocking collectives, body(): y = lax.all_to_all(y, 'tp', split_axis=0, concat_axis=1, tiled=True)  16.9 us
    pallas_call x1, Pallas kernels, mixers(): pl.pallas_call(functools.partial(mixers_kernel, tile), in_specs=[vmem()]...  12.5 us
    pallas_call x1, Pallas kernels, project(): pl.pallas_call(project_kernel, grid=(rows // tile,), in_specs=[pl.BlockSp...  9.54 us
    pallas_call x1, Pallas kernels, output(): pl.pallas_call(output_kernel, grid=(sp,), in_specs=[pl.BlockSpec((rows, k...  8.64 us
  transfers between devices with their start and end apart: 2, of which 0 were waited for; matrix products, arithmetic and copies ran while one was open for 7% of the time, Pallas kernels for 53%

profile of v2, /device:TPU:0, one launch (start us, length us, event | category | flops | bytes accessed | tf_op | source)
XLA Modules:
  0.0 173.3 jit_solution(3648096414728268909)
XLA Ops:
  6.5 0.0 all-gather.5.cloned.1.call-start
  6.5 1.7 pad_maximum_fusion.2
  8.2 0.0 all-gather.5.cloned.1.call-update
  8.3 1.3 broadcast_in_dim.24
  9.5 70.2 %gather.1 = bf16[8,256,1024]{2,1,0:T(8,128)(2,1)} custom-call(bf16[256,256]{1,0:T(8,128)(2,1)} %refs_0_.1, bf16[256,256]{1,0:T(8,128)(2,1)} %refs_1_.1, bf16[256,256]{1,0:T(8,128)(2,1)} %refs_2_.1, bf16[256,256]{1,0:T(8,128)(2,1)} %refs_3_.1), custom_call_target="tpu_custom_call" | custom-call | bytes 134217728 | tf_op jit(solution)/shard_map/gather/pallas_call | solution.py:149
  79.7 0.0 copy-start.1
  79.8 0.0 copy-start.2
  79.8 0.0 copy-start.5
  79.8 0.0 copy-start.3
  79.8 0.0 copy-start.4
  79.8 0.0 copy-start.6
  79.8 9.5 %project.1 = (f32[1024,256]{1,0:T(8,128)}, f32[1024,256]{1,0:T(8,128)}, f32[1024,256]{1,0:T(8,128)}) custom-call(bf16[1024,2048]{1,0:T(8,128)(2,1)} %x_ref.1, f32[1,2048]{1,0:T(1,128)} %bitcast.28, bf16[2048,1024]{1,0:T(8,128)(2,1)} %bitcast.25), custom_call_target="tpu_custom_call" | custom-call | flops 4294967296 | bytes 12582912 | tf_op jit(solution)/shard_map/project/pallas_call | solution.py:190
  89.4 0.8 slice.100
  90.1 0.8 slice.101
  90.9 2.6 %collective-permute-start = (bf16[32,512]{1,0:T(8,128)(2,1)S(1)}, bf16[32,512]{1,0:T(8,128)(2,1)S(1)}, u32[]{:S(2)}, u32[]{:S(2)}) collective-permute-start(bf16[32,512]{1,0:T(8,128)(2,1)S(1)} %pad_maximum_fusion.3), channel_id=1, source_target_pairs={{0,4},{4,8},{8,12},{12,16},{16,20},{20,24},{24,28},{1,5},{5,9},{9,... | collective-permute-start | bytes 98312 | tf_op jit(solution)/shard_map/ppermute | solution.py:371
  93.5 0.0 copy-done.1
  93.5 0.0 copy-done.2
  93.5 0.3 broadcast_multiply_fusion.1
  93.8 0.2 mul.101
  94.0 0.2 mul.98
  94.2 0.0 copy-done.5
  94.2 0.6 compare_select_fusion
  94.9 0.7 pad_maximum_fusion.1.maps_ref
  95.6 0.0 copy-done.3
  95.6 0.6 convert_element_type.26.taps_ref
  96.2 0.0 copy-done.4
  96.2 0.6 convert_element_type.27.short_ref
  96.8 0.0 copy-done.6
  96.8 0.6 broadcast_in_dim.25
  97.3 0.0 collective-permute-done
  97.3 0.6 fusion.1
  98.0 0.0 copy-start
  98.0 12.5 %mixers.1 = (bf16[1024,256]{1,0:T(8,128)(2,1)}, f32[1024,256]{1,0:T(8,128)}, f32[1024,256]{1,0:T(8,128)}, f32[2,256]{1,0:T(2,128)}) custom-call(f32[1024,256]{1,0:T(8,128)} %get-tuple-element.12.g_ref, f32[32,256]{1,0:T(8,128)} %get-tuple-element.20.gh_ref, f32[1024,256]{1,0:T(8,128)} %get-tuple-element.13.r_ref, f32[32,256]{1,0:T(8,128)} %get-tuple-element.19.rh_ref, ...), custom_call_target="tpu_custom_call" | custom-call | flops 3145728000 | bytes 8388608 | tf_op jit(solution)/shard_map/mixers/pallas_call | solution.py:315
  110.5 26.3 %all-gather.2 = f32[8,2,256]{2,1,0:T(2,128)S(1)} all-gather(f32[1,2,256]{2,1,0:T(2,128)} %bitcast.42), channel_id=2, replica_groups=mesh['sp'=8,'tp'=4] {'sp'}, dimensions={0}, use_global_device_ids=true | all-gather | bytes 18432 | tf_op jit(solution)/shard_map/all_gather | solution.py:418
  136.8 0.0 copy-done
  136.8 1.8 %multiply_convert_fusion = bf16[1024,256]{1,0:T(8,128)(2,1)S(1)} fusion(f32[1024,256]{1,0:T(8,128)S(1)} %copy-done, f32[1024,256]{1,0:T(8,128)} %get-tuple-element.15, f32[1024,256]{1,0:T(8,128)} %get-tuple-element.16, f32[256]{0:T(256)S(1)} %add_select_fusion), kind=kLoop, calls=%fused_computation.1 | loop fusion | flops 1048576 | bytes 3671040 | tf_op jit(solution)/shard_map/convert_element_type | solution.py:425
  138.6 1.1 pad_maximum_fusion
  139.7 16.9 %all_to_all.19 = bf16[4,256,512]{2,1,0:T(8,128)(2,1)S(1)} all-to-all(bf16[4,256,512]{2,1,0:T(8,128)(2,1)S(1)} %bitcast.26), channel_id=1, replica_groups=mesh['sp'=8,'tp'=4] {'tp'}, dimensions={0} | all-to-all | bytes 2097152 | tf_op jit(solution)/shard_map/all_to_all | solution.py:427
  156.6 1.2 copy.18
  157.8 0.0 all-gather.5.cloned.1.call-done
  157.8 8.6 %output.1 = bf16[256,2048]{1,0:T(8,128)(2,1)} custom-call(bf16[256,2048]{1,0:T(8,128)(2,1)} %bitcast.24, bf16[8,4,512,256]{3,2,1,0:T(8,128)(2,1)} %bitcast.23), custom_call_target="tpu_custom_call" | custom-call | tf_op jit(solution)/shard_map/output/pallas_call | solution.py:350
  (4 shorter events, 0.0 us)
Async XLA Ops:
  6.5 151.2 %all-gather.5.cloned.1.call-start = ((), (), s32[]{:S(2)}) async-start(), calls=%async_computation.1 | async-start | bytes 8650752 | tf_op jit(solution)/shard_map/all_gather | solution.py:398
  79.7 13.7 %copy-start.1 = (bf16[4,64,64]{2,1,0:T(8,128)(2,1)S(1)}, bf16[4,64,64]{2,1,0:T(8,128)(2,1)}, u32[]{:S(2)}) copy-start(bf16[4,64,64]{2,1,0:T(8,128)(2,1)} %param.24) | copy-start | bytes 98308
  79.8 13.7 %copy-start.2 = (bf16[4,64,64]{2,1,0:T(8,128)(2,1)S(1)}, bf16[4,64,64]{2,1,0:T(8,128)(2,1)}, u32[]{:S(2)}) copy-start(bf16[4,64,64]{2,1,0:T(8,128)(2,1)} %param.25) | copy-start | bytes 98308
  79.8 14.5 %copy-start.5 = (f32[256]{0:T(256)S(1)}, f32[256]{0:T(256)}, u32[]{:S(2)}) copy-start(f32[256]{0:T(256)} %param.26) | copy-start | bytes 3076
  79.8 15.8 %copy-start.3 = (bf16[31,256]{1,0:T(8,128)(2,1)S(1)}, bf16[31,256]{1,0:T(8,128)(2,1)}, u32[]{:S(2)}) copy-start(bf16[31,256]{1,0:T(8,128)(2,1)} %param.21) | copy-start | bytes 47620
  79.8 16.4 %copy-start.4 = (bf16[4,256]{1,0:T(4,128)(2,1)S(1)}, bf16[4,256]{1,0:T(4,128)(2,1)}, u32[]{:S(2)}) copy-start(bf16[4,256]{1,0:T(4,128)(2,1)} %param.23) | copy-start | bytes 6148
  79.8 17.0 %copy-start.6 = (bf16[256]{0:T(256)(128)(2,1)S(1)}, bf16[256]{0:T(256)(128)(2,1)}, u32[]{:S(2)}) copy-start(bf16[256]{0:T(256)(128)(2,1)} %param.22) | copy-start | bytes 1540
  90.9 6.5 %collective-permute-start = (bf16[32,512]{1,0:T(8,128)(2,1)S(1)}, bf16[32,512]{1,0:T(8,128)(2,1)S(1)}, u32[]{:S(2)}, u32[]{:S(2)}) collective-permute-start(bf16[32,512]{1,0:T(8,128)(2,1)S(1)} %pad_maximum_fusion.3), channel_id=1, source_target_pairs={{0,4},{4,8},{8,12},{12,16},{16,20},{20,24},{24,28},{1,5},{5,9},{9,... | collective-permute-start | bytes 98312 | tf_op jit(solution)/shard_map/ppermute | solution.py:371
  98.0 38.9 %copy-start = (f32[1024,256]{1,0:T(8,128)S(1)}, f32[1024,256]{1,0:T(8,128)}, u32[]{:S(2)}) copy-start(f32[1024,256]{1,0:T(8,128)} %get-tuple-element.18) | copy-start | bytes 3145732
Sparse Core Ops, SparseCore 0:
  10.2 85.0 all-gather.4

commit v3 on v2

--- a/solution.py
+++ b/solution.py
@@ -166,6 +166,54 @@
         ),
         name="gather",
     )(*parts)
+
+
+def spread_kernel(count, x_ref, out_ref, send, recv, local):
+    me = lax.axis_index("sp")
+
+    def peer(d):
+        return {"sp": (me + d) % count}
+
+    barrier = pltpu.get_barrier_semaphore()
+    kind = pl.DeviceIdType.MESH
+    for d in range(1, count):
+        pl.semaphore_signal(barrier, inc=1, device_id=peer(d), device_id_type=kind)
+    pl.semaphore_wait(barrier, count - 1)
+    own = pltpu.make_async_copy(x_ref, out_ref.at[me], local)
+    own.start()
+
+    def copy(d, slot):
+        return pltpu.make_async_remote_copy(
+            src_ref=x_ref,
+            dst_ref=out_ref.at[slot],
+            send_sem=send.at[d - 1],
+            recv_sem=recv.at[d - 1],
+            device_id=peer(d),
+            device_id_type=kind,
+        )
+
+    for d in range(1, count):
+        copy(d, me).start()
+    own.wait()
+    for d in range(1, count):
+        copy(d, (me + count - d) % count).wait_recv()
+        copy(d, me).wait_send()
+
+
+def spread_over(x, count):
+    return pl.pallas_call(
+        functools.partial(spread_kernel, count),
+        in_specs=[vmem()],
+        out_specs=vmem(),
+        out_shape=jax.ShapeDtypeStruct((count,) + x.shape, x.dtype),
+        scratch_shapes=[
+            pltpu.SemaphoreType.DMA((count - 1,)),
+            pltpu.SemaphoreType.DMA((count - 1,)),
+            pltpu.SemaphoreType.DMA,
+        ],
+        compiler_params=pltpu.CompilerParams(collective_id=1, has_side_effects=True),
+        name="spread",
+    )(x)
 
 
 def project_kernel(x_ref, gain_ref, w_ref, g_ref, r_ref, b_ref):
@@ -415,7 +463,7 @@
         maps,
         jax.nn.softplus(-rate_param)[None],
     )
-    lasts = lax.all_gather(last, "sp")
+    lasts = spread_over(last, sp)
     place = lax.axis_index("sp")
     incoming = jnp.zeros((c,), f32)
     for hop in range(sp - 1):

time: 174 us -> 156 us (0.90)
  blocking collectives: 43.2 us -> 16.9 us
  Pallas kernels: 101 us -> 109 us
    all_gather x1 -> x0, blocking collectives: 26.3 us -> none  [body(): lasts = lax.all_gather(last, 'sp')]
    pallas_call x0 -> x1, Pallas kernels: none -> 7.67 us  [spread_over(): pl.pallas_call(functools.partial(spread_kernel, count), in_specs=[vmem()]...]
  transfers between devices with their start and end apart: 2 -> 2, of which waited for: 0 -> 0; matrix products, arithmetic and copies ran while one was open for 7% -> 8% of each run, Pallas kernels for 53% -> 64%
where the time goes in v3:
time: 156 us; the launch traced here: 155 us
  Pallas kernels  109 us (70%)
  blocking collectives  16.9 us (11%)
  between operations  13.5 us (9%)
  other arithmetic  10.1 us (6%)
  local copies, waits for them, and re-layouts  3.82 us (2%)
  starting transfers between devices  2.56 us (2%)
    pallas_call x1, Pallas kernels, gather_input(): pl.pallas_call(functools.partial(gather_kernel, lines, width), in_specs=[...  70.2 us
    all_to_all x1, blocking collectives, body(): y = lax.all_to_all(y, 'tp', split_axis=0, concat_axis=1, tiled=True)  16.9 us
    pallas_call x1, Pallas kernels, mixers(): pl.pallas_call(functools.partial(mixers_kernel, tile), in_specs=[vmem()]...  12.5 us
    pallas_call x1, Pallas kernels, project(): pl.pallas_call(project_kernel, grid=(rows // tile,), in_specs=[pl.BlockSp...  9.54 us
    pallas_call x1, Pallas kernels, output(): pl.pallas_call(output_kernel, grid=(sp,), in_specs=[pl.BlockSpec((rows, k...  8.64 us
    pallas_call x1, Pallas kernels, spread_over(): pl.pallas_call(functools.partial(spread_kernel, count), in_specs=[vmem()]...  7.67 us
  transfers between devices with their start and end apart: 2, of which 0 were waited for; matrix products, arithmetic and copies ran while one was open for 8% of the time, Pallas kernels for 64%

profile of v3, /device:TPU:0, one launch (start us, length us, event | category | flops | bytes accessed | tf_op | source)
XLA Modules:
  0.0 155.4 jit_solution(16996332223163364431)
XLA Ops:
  6.5 0.0 all-gather.3.cloned.1.call-start
  6.5 1.7 %pad_maximum_fusion.2 = bf16[512,256]{1,0:T(8,128)(2,1)} fusion(bf16[256,256]{1,0:T(8,128)(2,1)} %param.29, bf16[256,256]{1,0:T(8,128)(2,1)} %param.28), kind=kLoop, calls=%fused_computation.3 | loop fusion | flops 524288 | bytes 524288 | tf_op jit(solution)/shard_map/concatenate | solution.py:445
  8.2 0.0 all-gather.3.cloned.1.call-update
  8.3 1.3 broadcast_in_dim.24
  9.5 70.2 %gather.1 = bf16[8,256,1024]{2,1,0:T(8,128)(2,1)} custom-call(bf16[256,256]{1,0:T(8,128)(2,1)} %refs_0_.1, bf16[256,256]{1,0:T(8,128)(2,1)} %refs_1_.1, bf16[256,256]{1,0:T(8,128)(2,1)} %refs_2_.1, bf16[256,256]{1,0:T(8,128)(2,1)} %refs_3_.1), custom_call_target="tpu_custom_call" | custom-call | bytes 134217728 | tf_op jit(solution)/shard_map/gather/pallas_call | solution.py:149
  79.7 0.0 copy-start.1
  79.8 0.0 copy-start.2
  79.8 0.0 copy-start.5
  79.8 0.0 copy-start.3
  79.8 0.0 copy-start.4
  79.8 0.0 copy-start.6
  79.8 9.5 %project.1 = (f32[1024,256]{1,0:T(8,128)}, f32[1024,256]{1,0:T(8,128)}, f32[1024,256]{1,0:T(8,128)}) custom-call(bf16[1024,2048]{1,0:T(8,128)(2,1)} %x_ref.1, f32[1,2048]{1,0:T(1,128)} %bitcast.27, bf16[2048,1024]{1,0:T(8,128)(2,1)} %bitcast.24), custom_call_target="tpu_custom_call" | custom-call | flops 4294967296 | bytes 12582912 | tf_op jit(solution)/shard_map/project/pallas_call | solution.py:238
  89.4 0.8 slice.82
  90.1 0.8 slice.83
  90.9 2.6 %collective-permute-start = (bf16[32,512]{1,0:T(8,128)(2,1)S(1)}, bf16[32,512]{1,0:T(8,128)(2,1)S(1)}, u32[]{:S(2)}, u32[]{:S(2)}) collective-permute-start(bf16[32,512]{1,0:T(8,128)(2,1)S(1)} %pad_maximum_fusion.3), channel_id=1, source_target_pairs={{0,4},{4,8},{8,12},{12,16},{16,20},{20,24},{24,28},{1,5},{5,9},{9,... | collective-permute-start | bytes 98312 | tf_op jit(solution)/shard_map/ppermute | solution.py:419
  93.5 0.0 copy-done.1
  93.5 0.0 copy-done.2
  93.5 0.3 broadcast_multiply_fusion.1
  93.8 0.2 mul.101
  94.0 0.2 mul.98
  94.2 0.0 copy-done.5
  94.2 0.6 compare_select_fusion
  94.9 0.7 pad_maximum_fusion.1.maps_ref
  95.6 0.0 copy-done.3
  95.6 0.6 convert_element_type.26.taps_ref
  96.2 0.0 copy-done.4
  96.2 0.6 convert_element_type.27.short_ref
  96.8 0.0 copy-done.6
  96.8 0.6 broadcast_in_dim.25
  97.3 0.0 collective-permute-done
  97.3 0.6 fusion.1
  98.0 0.0 copy-start
  98.0 12.5 %mixers.1 = (bf16[1024,256]{1,0:T(8,128)(2,1)}, f32[1024,256]{1,0:T(8,128)}, f32[1024,256]{1,0:T(8,128)}, f32[2,256]{1,0:T(2,128)}) custom-call(f32[1024,256]{1,0:T(8,128)} %get-tuple-element.12.g_ref, f32[32,256]{1,0:T(8,128)} %get-tuple-element.20.gh_ref, f32[1024,256]{1,0:T(8,128)} %get-tuple-element.13.r_ref, f32[32,256]{1,0:T(8,128)} %get-tuple-element.19.rh_ref, ...), custom_call_target="tpu_custom_call" | custom-call | flops 3145728000 | bytes 8388608 | tf_op jit(solution)/shard_map/mixers/pallas_call | solution.py:363
  110.5 7.7 %spread.1 = f32[8,2,256]{2,1,0:T(2,128)} custom-call(f32[2,256]{1,0:T(2,128)} %get-tuple-element.17.x_ref), custom_call_target="tpu_custom_call" | custom-call | tf_op jit(solution)/shard_map/spread/pallas_call | solution.py:204
  118.1 0.8 fusion.2
  119.0 0.0 copy-done
  119.0 1.8 %multiply_convert_fusion = bf16[1024,256]{1,0:T(8,128)(2,1)S(1)} fusion(f32[1024,256]{1,0:T(8,128)S(1)} %copy-done, f32[1024,256]{1,0:T(8,128)} %get-tuple-element.15, f32[1024,256]{1,0:T(8,128)} %get-tuple-element.16, f32[256]{0:T(256)S(1)} %add_select_fusion), kind=kLoop, calls=%fused_computation.1 | loop fusion | flops 1048576 | bytes 3671040 | tf_op jit(solution)/shard_map/convert_element_type | solution.py:473
  120.7 1.1 pad_maximum_fusion
  121.9 16.9 %all_to_all.19 = bf16[4,256,512]{2,1,0:T(8,128)(2,1)S(1)} all-to-all(bf16[4,256,512]{2,1,0:T(8,128)(2,1)S(1)} %bitcast.25), channel_id=1, replica_groups=mesh['sp'=8,'tp'=4] {'tp'}, dimensions={0} | all-to-all | bytes 2097152 | tf_op jit(solution)/shard_map/all_to_all | solution.py:475
  138.7 1.2 copy.18
  139.9 0.0 all-gather.3.cloned.1.call-done
  139.9 8.6 %output.1 = bf16[256,2048]{1,0:T(8,128)(2,1)} custom-call(bf16[256,2048]{1,0:T(8,128)(2,1)} %bitcast.23, bf16[8,4,512,256]{3,2,1,0:T(8,128)(2,1)} %bitcast.22), custom_call_target="tpu_custom_call" | custom-call | tf_op jit(solution)/shard_map/output/pallas_call | solution.py:398
  (3 shorter events, 0.0 us)
Async XLA Ops:
  6.5 133.4 %all-gather.3.cloned.1.call-start = ((), (), s32[]{:S(2)}) async-start(), calls=%async_computation.1 | async-start | bytes 8650752 | tf_op jit(solution)/shard_map/all_gather | solution.py:446
  79.7 13.7 %copy-start.1 = (bf16[4,64,64]{2,1,0:T(8,128)(2,1)S(1)}, bf16[4,64,64]{2,1,0:T(8,128)(2,1)}, u32[]{:S(2)}) copy-start(bf16[4,64,64]{2,1,0:T(8,128)(2,1)} %param.24) | copy-start | bytes 98308
  79.8 13.7 %copy-start.2 = (bf16[4,64,64]{2,1,0:T(8,128)(2,1)S(1)}, bf16[4,64,64]{2,1,0:T(8,128)(2,1)}, u32[]{:S(2)}) copy-start(bf16[4,64,64]{2,1,0:T(8,128)(2,1)} %param.25) | copy-start | bytes 98308
  79.8 14.5 %copy-start.5 = (f32[256]{0:T(256)S(1)}, f32[256]{0:T(256)}, u32[]{:S(2)}) copy-start(f32[256]{0:T(256)} %param.26) | copy-start | bytes 3076
  79.8 15.8 %copy-start.3 = (bf16[31,256]{1,0:T(8,128)(2,1)S(1)}, bf16[31,256]{1,0:T(8,128)(2,1)}, u32[]{:S(2)}) copy-start(bf16[31,256]{1,0:T(8,128)(2,1)} %param.21) | copy-start | bytes 47620
  79.8 16.4 %copy-start.4 = (bf16[4,256]{1,0:T(4,128)(2,1)S(1)}, bf16[4,256]{1,0:T(4,128)(2,1)}, u32[]{:S(2)}) copy-start(bf16[4,256]{1,0:T(4,128)(2,1)} %param.23) | copy-start | bytes 6148
  79.8 17.0 %copy-start.6 = (bf16[256]{0:T(256)(128)(2,1)S(1)}, bf16[256]{0:T(256)(128)(2,1)}, u32[]{:S(2)}) copy-start(bf16[256]{0:T(256)(128)(2,1)} %param.22) | copy-start | bytes 1540
  90.9 6.5 %collective-permute-start = (bf16[32,512]{1,0:T(8,128)(2,1)S(1)}, bf16[32,512]{1,0:T(8,128)(2,1)S(1)}, u32[]{:S(2)}, u32[]{:S(2)}) collective-permute-start(bf16[32,512]{1,0:T(8,128)(2,1)S(1)} %pad_maximum_fusion.3), channel_id=1, source_target_pairs={{0,4},{4,8},{8,12},{12,16},{16,20},{20,24},{24,28},{1,5},{5,9},{9,... | collective-permute-start | bytes 98312 | tf_op jit(solution)/shard_map/ppermute | solution.py:419
  98.0 21.0 %copy-start = (f32[1024,256]{1,0:T(8,128)S(1)}, f32[1024,256]{1,0:T(8,128)}, u32[]{:S(2)}) copy-start(f32[1024,256]{1,0:T(8,128)} %get-tuple-element.18) | copy-start | bytes 3145732
Sparse Core Ops, SparseCore 0:
  10.2 85.0 all-gather.2
